TPU v7x, 32 devices: a whole 2x2x4 slice. The times are simulated.
32 devices in a mesh: sp: 8 (over z, x), tp: 4 (over y, core).
Axes of the slice: x: 2, y: 2, z: 4, core: 2. Of those that a mesh axis runs over, the one named last changes fastest.
Arguments:
- tokens: bfloat16 [8192, 2048], P('sp'), may hold values from -8 to 8
- norm_gain: float32 [2048], replicated, may hold values from 0.1 to 1.9
- query_weight: bfloat16 [2048, 512], P(None, 'tp'), may hold values from -40 to 40
- key_weight: bfloat16 [2048, 256], P(None, 'tp'), may hold values from -1 to 1
- value_weight: bfloat16 [2048, 256], P(None, 'tp'), may hold values from -0.125 to 0.125
- sink_logits: float32 [8], P('tp'), may hold values from 1 to 6
- conv_in_weight: bfloat16 [2048, 512], P(None, 'tp'), may hold values from -0.125 to 0.125
- conv_gate_weight: bfloat16 [2048, 512], P(None, 'tp'), may hold values from -0.125 to 0.125
- conv_taps: bfloat16 [31, 512], replicated, may hold values from -1 to 1
- conv_gain: float32 [512], replicated, may hold values from 0.1 to 1.9
- point_weight: bfloat16 [512, 512], replicated, may hold values from -0.25 to 0.25
- output_gain: float32 [1024], replicated, may hold values from 0.1 to 1.9
- output_weight: bfloat16 [1024, 2048], P('sp'), may hold values from -0.1875 to 0.1875
Outputs:
- mixed_output: bfloat16 [8192, 2048], P(('sp', 'tp'))
All inputs are finite; a program needn't handle non-finite values.
Results may differ from a plain program's by a relative error of at most 0.0087.
Values may be sent and summed in bfloat16 or wider, within the bound.
A program may use at most 64 MiB of HBM per device.

v0:
```python
import functools

import jax
import jax.numpy as jnp
from jax import lax
from jax.experimental import pallas as pl
from jax.experimental.pallas import tpu as pltpu
from jax.sharding import PartitionSpec as P

HEAD_DIM = 64
WINDOW = 128
CONV_WIDTH = 31
HALO = 32
EPS = 1e-06
MASKED = -1e30
F32 = jnp.float32
BF16 = jnp.bfloat16
MESH = pl.DeviceIdType.MESH


def kernel(
    S, T,
    tok_hbm, ng, qw, kw, vw, sink, iw, gw, taps, cg, pw_hbm, og, ow_hbm,
    out,
    tok, wcat, kvs, pw, wfull, qb, kvb, g, a, ar, gr, ext, conv, act, mg,
    lsem, zsend, osend, psend, xsend, ysend, csend, wrecv, hsend, hrecv, asend, arecv, gsend, grecv,
):
    s, t = lax.axis_index("sp"), lax.axis_index("tp")
    R, D = tok.shape
    Q = R // T
    Kl = ow_hbm.shape[0]
    Y, Z = T // 2, S // 2
    z, x = s // 2, lax.rem(s, 2)
    y, c = t // 2, lax.rem(t, 2)
    CC = g.shape[1]
    HW = a.shape[1]

    own = pl.ds(pl.multiple_of(s * Kl, Kl), Kl)
    loads = [pltpu.make_async_copy(ow_hbm, wfull.at[own], lsem.at[0])]
    loads += [
        pltpu.make_async_copy(qw, wcat.at[:, 0:HW], lsem.at[1]),
        pltpu.make_async_copy(kw, kvs.at[0 : kw.shape[0]], lsem.at[2]),
        pltpu.make_async_copy(vw, kvs.at[kw.shape[0] : 2 * kw.shape[0]], lsem.at[3]),
        pltpu.make_async_copy(iw, wcat.at[:, 2 * HW : 2 * HW + CC], lsem.at[4]),
        pltpu.make_async_copy(gw, wcat.at[:, 2 * HW + CC : 2 * HW + 2 * CC], lsem.at[5]),
        pltpu.make_async_copy(pw_hbm, pw, lsem.at[6]),
    ]
    tloads = [
        pltpu.make_async_copy(tok_hbm.at[q * Q : (q + 1) * Q], tok.at[q * Q : (q + 1) * Q], lsem.at[7 + q])
        for q in range(T)
    ]
    loads[0].start()
    tloads[T - 1].start()
    for i in range(1, 6):
        loads[i].start()
    for q in range(T - 2, -1, -1):
        tloads[q].start()
    loads[6].start()

    bar = pltpu.get_barrier_semaphore()

    def hello(ds_, dt_):
        pl.semaphore_signal(bar, inc=1, device_id=(ds_, dt_), device_id_type=MESH)

    for d in range(1, T):
        hello(s, lax.rem(t + d, T))
    hello(s + 1 - 2 * x, t)
    for step in (1, 2):
        @pl.when(s >= step)
        def _():
            hello(s - step, t)

        @pl.when(s + step < S)
        def _():
            hello(s + step, t)

    peers = T
    for step in (1, 2):
        peers = peers + jnp.where(s >= step, 1, 0) + jnp.where(s + step < S, 1, 0)
    pl.semaphore_wait(bar, peers)

    half, wide = D // 2, D // 4
    narrow = wide // Y
    other_x = s + 1 - 2 * x
    sib = y * 2 + 1 - c

    def piece(sh, cc, j):
        rows = pl.ds(pl.multiple_of(sh * Kl, Kl), Kl)
        if j is None:
            return wfull.at[rows, pl.ds(pl.multiple_of(cc * half, wide), wide)]
        return wfull.at[rows, pl.ds(pl.multiple_of(cc * half + wide + j * narrow, narrow), narrow)]

    def slot(cc, j):
        return cc * (Y + 1) + (0 if j is None else 1 + j)

    def send(sh, j, ds_, dt_, sem):
        ref = piece(sh, c, j)
        pltpu.make_async_remote_copy(
            src_ref=ref, dst_ref=ref, send_sem=sem, recv_sem=wrecv.at[sh, slot(c, j)],
            device_id=(ds_, dt_), device_id_type=MESH,
        ).start()

    def got(sh, cc, j):
        ref = piece(sh, cc, j)
        pltpu.make_async_copy(ref, ref, wrecv.at[sh, slot(cc, j)]).wait()

    def sent(j, sem):
        ref = piece(0, 0, j)
        pltpu.make_async_copy(ref, ref, sem).wait()

    def yplane(k):
        return lax.rem(y + k, Y)

    def both(d):
        return ((z >= d, z - d, z + 1 < Z, 2), (z + d < Z, z + d, z >= 1, -2))

    def z_both(sh, j, i):
        @pl.when(z + 1 < Z)
        def _():
            send(sh, j, s + 2, t, zsend.at[z, i])

        @pl.when(z >= 1)
        def _():
            send(sh, j, s - 2, t, osend.at[i])

    def across_y(sh, zz, i):
        for k in range(1, Y):
            send(sh, y, s, yplane(k) * 2 + c, ysend.at[zz, i * (Y - 1) + k - 1])

    def z_own():
        send(s, y, other_x, t, psend.at[0])
        z_both(s, None, 0)
        send(s, None, other_x, t, xsend.at[z])
        z_both(s, y, 1)

    def crossed():
        got(other_x, c, y)
        z_both(other_x, y, 2)
        across_y(other_x, z, 1)
        send(other_x, y, s, sib, csend.at[z, Y + 2])

    def z_step(d, i):
        for ok, zz, more, hop in both(d):
            @pl.when(ok)
            def _():
                sh = zz * 2 + (1 - x if i == 2 else x)
                j = None if i == 0 else y
                got(sh, c, j)

                @pl.when(more)
                def _():
                    send(sh, j, s + hop, t, zsend.at[zz, i])

                if i == 0:
                    send(sh, j, other_x, t, xsend.at[zz])
                    send(sh, j, s, sib, csend.at[zz, 0])
                else:
                    across_y(sh, zz, i - 1)
                    send(sh, j, s, sib, csend.at[zz, (i - 1) * (Y + 1) + 1])

    def at_distance(d, one):
        if d == 0:
            one(z)
        else:
            for ok, zz, _, _ in both(d):
                @pl.when(ok)
                def _():
                    one(zz)

    def x_one(zz):
        sh = zz * 2 + 1 - x
        got(sh, c, None)
        send(sh, None, s, sib, csend.at[zz, Y + 1])

    def y_one(d):
        def one(zz):
            for i in ((1,) if d == 0 else (0, 1)):
                sh = zz * 2 + (x if i == 0 else 1 - x)
                for k in range(1, Y):
                    got(sh, c, yplane(k))
                    send(sh, yplane(k), s, sib, csend.at[zz, i * (Y + 1) + 1 + k])
        at_distance(d, one)

    events = [crossed]
    for d in range(1, Z + 1):
        if d < Z:
            for i in range(3):
                events.append(functools.partial(z_step, d, i))
        events.append(functools.partial(at_distance, d - 1, x_one))
        events.append(functools.partial(y_one, d - 1))

    loads[0].wait()
    z_own()

    for i in range(1, 6):
        loads[i].wait()
    wcat[:, HW : 2 * HW] = kvs[...].T

    def send_gated(q):
        rows = pl.ds(q * Q, HALO + Q)

        @pl.when(t != q)
        def _():
            pltpu.make_async_remote_copy(
                src_ref=g.at[rows], dst_ref=gr.at[t], send_sem=gsend.at[q], recv_sem=grecv.at[t],
                device_id=(s, q), device_id_type=MESH,
            ).start()

    def halo(ref, n, i):
        return pltpu.make_async_remote_copy(
            src_ref=ref.at[pl.ds(R, n)], dst_ref=ref.at[pl.ds(0, n)],
            send_sem=hsend.at[i], recv_sem=hrecv.at[i],
            device_id=(lax.rem(s + 1, S), t), device_id_type=MESH,
        )

    def run(n):
        for _ in range(n):
            if events:
                events.pop(0)()

    for q in range(T - 1, -1, -1):
        tloads[q].wait()
        xs = tok[q * Q : (q + 1) * Q, :].astype(F32)
        scale = lax.rsqrt(jnp.mean(xs * xs, axis=-1, keepdims=True) + EPS)
        normed = (xs * scale * ng[...]).astype(BF16)
        p = jnp.dot(normed, wcat[...], preferred_element_type=F32)
        qb[q * Q : (q + 1) * Q, :] = (p[:, :HW] * HEAD_DIM ** (-0.5)).astype(BF16)
        kvb[WINDOW + q * Q : WINDOW + (q + 1) * Q, :] = p[:, HW : 2 * HW].astype(BF16)
        g[HALO + q * Q : HALO + (q + 1) * Q, :] = (
            p[:, 2 * HW : 2 * HW + CC] * jax.nn.sigmoid(p[:, 2 * HW + CC :])
        ).astype(BF16)
        if q == T - 1:
            @pl.when(s + 1 < S)
            def _():
                halo(kvb, WINDOW, 0).start()
                halo(g, HALO, 1).start()
        else:
            send_gated(q + 1)
        run(1 if q == T - 1 else 2 if q < T - 2 else 1)

    @pl.when(s == 0)
    def _():
        kvb[0:WINDOW, :] = jnp.zeros((WINDOW, kvb.shape[1]), BF16)
        g[0:HALO, :] = jnp.zeros((HALO, CC), BF16)

    @pl.when(s > 0)
    def _():
        halo(kvb, WINDOW, 0).wait_recv()
        halo(g, HALO, 1).wait_recv()

    send_gated(0)

    row = lax.broadcasted_iota(jnp.int32, (2 * WINDOW, 2 * WINDOW), 0)
    col = lax.broadcasted_iota(jnp.int32, (2 * WINDOW, 2 * WINDOW), 1)
    dist = WINDOW + lax.rem(row, WINDOW) - col
    inside = (dist >= 0) & (dist < WINDOW)
    head = lax.broadcasted_iota(jnp.int32, (2 * WINDOW, 1), 0) < WINDOW
    sinks = jnp.where(head, sink[0], sink[1])
    for i in range(T):
        q = lax.rem(t + 1 + i, T)
        for b in range(Q // WINDOW):
            base = pl.multiple_of(q * Q + b * WINDOW, WINDOW)
            rows = qb[pl.ds(base, WINDOW), :]
            kv = kvb[pl.ds(base, 2 * WINDOW), :]
            q2 = jnp.concatenate([rows[:, :HEAD_DIM], rows[:, HEAD_DIM:]], axis=0)
            sc = lax.dot_general(
                q2, kv[:, :HEAD_DIM], (((1,), (1,)), ((), ())), preferred_element_type=F32
            )
            low = jnp.where((s == 0) & (base == 0), WINDOW, 0)
            sc = jnp.where(inside & (col >= low), sc, MASKED)
            top = jnp.maximum(jnp.max(sc, axis=-1, keepdims=True), sinks)
            e = jnp.exp(sc - top)
            den = jnp.sum(e, axis=-1, keepdims=True) + jnp.exp(sinks - top)
            w = (e * (1.0 / den)).astype(BF16)
            o = jnp.dot(w, kv[:, HEAD_DIM:], preferred_element_type=F32).astype(BF16)
            a[pl.ds(base, WINDOW), :] = jnp.concatenate([o[:WINDOW], o[WINDOW:]], axis=1)
        if i < T - 1:
            pltpu.make_async_remote_copy(
                src_ref=a.at[pl.ds(pl.multiple_of(q * Q, Q), Q)], dst_ref=ar.at[t],
                send_sem=asend.at[i], recv_sem=arecv.at[t],
                device_id=(s, q), device_id_type=MESH,
            ).start()
        run(2)
    mine = pl.multiple_of(t * Q, Q)
    ar[t] = a[pl.ds(mine, Q), :]
    gr[t] = g[pl.ds(mine, HALO + Q), :]
    run(1)

    first = HALO - (CONV_WIDTH - 1)
    for d in range(1, T):
        p = lax.rem(t + d, T)
        pltpu.make_async_copy(gr.at[p], gr.at[p], grecv.at[p]).wait()
    total = jnp.zeros((Q, 1), F32)
    for p in range(T):
        ext[p] = gr[p].astype(F32)
        acc = jnp.zeros((Q, CC), F32)
        tp = taps[:, p * CC : (p + 1) * CC].astype(F32)
        for k in range(CONV_WIDTH):
            acc = acc + tp[k : k + 1] * ext[p, first + k : first + k + Q, :]
        rounded = acc.astype(BF16)
        conv[:, p * CC : (p + 1) * CC] = rounded
        if p == 1:
            run(1)
    run(1)
    cv = conv[...].astype(F32)
    cen = cv - jnp.mean(cv, axis=-1, keepdims=True)
    norm = cen * lax.rsqrt(jnp.mean(cen * cen, axis=-1, keepdims=True) + EPS) * cg[...]
    act[...] = (norm * jax.nn.sigmoid(norm)).astype(BF16)
    loads[6].wait()
    pt = jnp.dot(act[...], pw[...], preferred_element_type=F32)
    AW = T * HW
    mg[:, AW:] = (
        pt * lax.rsqrt(jnp.mean(pt * pt, axis=-1, keepdims=True) + EPS) * og[:, AW:]
    ).astype(BF16)
    run(1)
    for d in range(1, T):
        p = lax.rem(t + d, T)
        pltpu.make_async_copy(ar.at[p], ar.at[p], arecv.at[p]).wait()
    heads = jnp.concatenate([ar[p] for p in range(T)], axis=1).astype(F32)
    mg[:, :AW] = (
        heads * lax.rsqrt(jnp.mean(heads * heads, axis=-1, keepdims=True) + EPS) * og[:, :AW]
    ).astype(BF16)

    run(len(events))
    for d in range(Z):
        def rest(zz):
            for j in (None, *range(Y)):
                if d > 0:
                    got(zz * 2 + x, 1 - c, j)
                got(zz * 2 + 1 - x, 1 - c, j)
        at_distance(d, rest)

    nb = 512
    for n in range(D // nb):
        out[:, n * nb : (n + 1) * nb] = jnp.dot(
            mg[...], wfull[:, n * nb : (n + 1) * nb], preferred_element_type=F32
        ).astype(BF16)

    sent(0, psend.at[0])
    for i in range(3):
        j = None if i == 0 else 0

        @pl.when(z + 1 < Z)
        def _():
            sent(j, zsend.at[z, i])

        @pl.when(z >= 1)
        def _():
            sent(j, osend.at[i])

    for d in range(1, Z):
        for ok, zz, more, _ in both(d):
            @pl.when(ok & more)
            def _():
                for i in range(3):
                    sent(None if i == 0 else 0, zsend.at[zz, i])

    for d in range(Z):
        def done(zz):
            sent(None, xsend.at[zz])
            for i in ((1,) if d == 0 else (0, 1)):
                for k in range(1, Y):
                    sent(0, ysend.at[zz, i * (Y - 1) + k - 1])
                for k in range(Y + 1):
                    sent(None if k == 0 else 0, csend.at[zz, i * (Y + 1) + k])
        at_distance(d, done)

    @pl.when(s + 1 < S)
    def _():
        halo(kvb, WINDOW, 0).wait_send()
        halo(g, HALO, 1).wait_send()

    for q in range(T):
        @pl.when(t != q)
        def _():
            pltpu.make_async_copy(gr.at[0], gr.at[0], gsend.at[q]).wait()
    for i in range(T - 1):
        pltpu.make_async_copy(ar.at[0], ar.at[0], asend.at[i]).wait()


def solution(mesh):
    S, T = mesh.shape["sp"], mesh.shape["tp"]

    def step(
        tokens, norm_gain, query_weight, key_weight, value_weight, sink_logits, conv_in_weight,
        conv_gate_weight, conv_taps, conv_gain, point_weight, output_gain, output_weight,
    ):
        R, D = tokens.shape
        Q = R // T
        HW, KW, CC = query_weight.shape[1], key_weight.shape[1], conv_in_weight.shape[1]
        C = point_weight.shape[0]
        MIX = output_gain.shape[0]
        Y, Z = T // 2, S // 2
        hbm = pl.BlockSpec(memory_space=pl.ANY)
        vmem = pl.BlockSpec(memory_space=pltpu.VMEM)
        smem = pl.BlockSpec(memory_space=pltpu.SMEM)
        dma = pltpu.SemaphoreType.DMA
        return pl.pallas_call(
            functools.partial(kernel, S, T),
            out_shape=jax.ShapeDtypeStruct((Q, D), BF16),
            in_specs=[hbm, vmem, hbm, hbm, hbm, smem, hbm, hbm, vmem, vmem, hbm, vmem, hbm],
            out_specs=vmem,
            scratch_shapes=[
                pltpu.VMEM((R, D), BF16),
                pltpu.VMEM((D, HW + 2 * KW + 2 * CC), BF16),
                pltpu.VMEM((2 * KW, D), BF16),
                pltpu.VMEM((C, C), BF16),
                pltpu.VMEM((MIX, D), BF16),
                pltpu.VMEM((R, HW), BF16),
                pltpu.VMEM((R + WINDOW, 2 * KW), BF16),
                pltpu.VMEM((R + HALO, CC), BF16),
                pltpu.VMEM((R, HW), BF16),
                pltpu.VMEM((T, Q, HW), BF16),
                pltpu.VMEM((T, Q + HALO, CC), BF16),
                pltpu.VMEM((T, Q + HALO, CC), F32),
                pltpu.VMEM((Q, C), BF16),
                pltpu.VMEM((Q, C), BF16),
                pltpu.VMEM((Q, MIX), BF16),
                dma((7 + T,)),
                dma((Z, 3)),
                dma((3,)),
                dma((1,)),
                dma((Z,)),
                dma((Z, 2 * (Y - 1))),
                dma((Z, 2 * (Y + 1))),
                dma((S, 2 * (Y + 1))),
                dma((2,)),
                dma((2,)),
                dma((T,)),
                dma((T,)),
                dma((T,)),
                dma((T,)),
            ],
            compiler_params=pltpu.CompilerParams(
                collective_id=0, has_side_effects=True, vmem_limit_bytes=56 * 1024 * 1024
            ),
        )(
            tokens, norm_gain[None], query_weight, key_weight.T, value_weight.T, sink_logits,
            conv_in_weight, conv_gate_weight, conv_taps, conv_gain[None], point_weight,
            output_gain[None], output_weight,
        )

    in_specs = (
        P("sp", None), P(), P(None, "tp"), P(None, "tp"), P(None, "tp"), P("tp"), P(None, "tp"),
        P(None, "tp"), P(), P(), P(), P(), P("sp", None),
    )
    return jax.shard_map(
        step, mesh=mesh, in_specs=in_specs, out_specs=P(("sp", "tp"), None), check_vma=False
    )
```

profile of v0, /device:TPU:1, one launch (start us, length us, event | category | flops | bytes accessed | tf_op | source)
XLA Modules:
  0.0 33.5 jit_solution(857915333528263989)
XLA Ops:
  0.0 31.2 %shard_map.127 = bf16[256,2048]{1,0:T(8,128)(2,1)} custom-call(bf16[1024,2048]{1,0:T(8,128)(2,1)} %tok_hbm.1, f32[1,2048]{1,0:T(1,128)} %bitcast.7, bf16[2048,128]{1,0:T(8,128)(2,1)} %qw.1, bf16[64,2048]{1,0:T(8,128)(2,1)} %bitcast.5, bf16[64,2048]{1,0:T(8,128)(2,1)} %bitcast.6, f32[2]{0:T(128)} %sink.1, bf16[2048,128]{1,0:T(8,128)(2,1)} %iw.1, ...), custom_call_target="tpu_custom_call" | custom-call | tf_op jit(solution)/shard_map/pallas_call | solution.py:398
  31.2 2.3 %copy.15 = bf16[256,2048]{1,0:T(8,128)(2,1)} copy(bf16[256,2048]{1,0:T(8,128)(2,1)} %shard_map.127) | data formatting | bytes 2097152
where the time goes:
time: 33.7 us; the launch traced here: 33.5 us
  Pallas kernels  31.2 us (93%)
  local copies, waits for them, and re-layouts  2.3 us (7%)
    pallas_call x1, Pallas kernels, step(): pl.pallas_call(functools.partial(kernel, S, T), out_shape=jax.ShapeDtypeS...  31.2 us
    unnamed x1, local copies, waits for them, and re-layouts  2.3 us

commit v1 on v0

v1 whole, which is shorter than its diff:
```python
import functools

import jax
import jax.numpy as jnp
from jax import lax
from jax.experimental import pallas as pl
from jax.experimental.pallas import tpu as pltpu
from jax.sharding import PartitionSpec as P

HEAD_DIM = 64
WINDOW = 128
CONV_WIDTH = 31
HALO = 32
EPS = 1e-06
MASKED = -1e30
F32 = jnp.float32
BF16 = jnp.bfloat16
MESH = pl.DeviceIdType.MESH


def kernel(
    S, T,
    tok_hbm, ng_hbm, qw, kw, vw, sink_hbm, iw, gw, taps_hbm, cg_hbm, pw_hbm, og_hbm, ow_hbm,
    out,
    tok, wcat, kvs, pw, wfull, qb, kvb, g, a, ar, gr, ext, conv, act, mg, acc, theirs, ng, sink, taps, cg, og,
    lsem, wsend, wrecv, hsend, hrecv, asend, arecv, gsend, grecv, msend, mrecv, osend, orecv,
):
    s, t = lax.axis_index("sp"), lax.axis_index("tp")
    R, D = tok.shape
    Q = R // T
    Kl = ow_hbm.shape[0]
    Y, Z = T // 2, S // 2
    z, x = s // 2, lax.rem(s, 2)
    y, c = t // 2, lax.rem(t, 2)
    CC = g.shape[1]
    HW = a.shape[1]

    half, wide = D // 2, D // 4
    part, narrow = wide // 2, wide // Y
    own = pl.ds(pl.multiple_of(s * Kl, Kl), Kl)
    own_half = ow_hbm.at[:, pl.ds(pl.multiple_of(c * half, half), half)]
    loads = [pltpu.make_async_copy(own_half, wfull.at[own], lsem.at[0])]
    loads += [
        pltpu.make_async_copy(qw, wcat.at[:, 0:HW], lsem.at[1]),
        pltpu.make_async_copy(kw, kvs.at[0 : kw.shape[0]], lsem.at[2]),
        pltpu.make_async_copy(vw, kvs.at[kw.shape[0] : 2 * kw.shape[0]], lsem.at[3]),
        pltpu.make_async_copy(iw, wcat.at[:, 2 * HW : 2 * HW + CC], lsem.at[4]),
        pltpu.make_async_copy(gw, wcat.at[:, 2 * HW + CC : 2 * HW + 2 * CC], lsem.at[5]),
        pltpu.make_async_copy(pw_hbm, pw, lsem.at[6]),
    ]
    tloads = [
        pltpu.make_async_copy(tok_hbm.at[q * Q : (q + 1) * Q], tok.at[q * Q : (q + 1) * Q], lsem.at[7 + q])
        for q in range(T)
    ]
    bar = pltpu.get_barrier_semaphore()

    def hello(ds_, dt_):
        pl.semaphore_signal(bar, inc=1, device_id=(ds_, dt_), device_id_type=MESH)

    for d in range(1, T):
        hello(s, lax.rem(t + d, T))
    hello(s + 1 - 2 * x, t)
    peers = T
    for step in (1, 2):
        @pl.when(s >= step)
        def _():
            hello(s - step, t)

        @pl.when(s + step < S)
        def _():
            hello(s + step, t)

        peers = peers + jnp.where(s >= step, 1, 0) + jnp.where(s + step < S, 1, 0)
    small = [
        pltpu.make_async_copy(src, dst, lsem.at[7 + T + i])
        for i, (src, dst) in enumerate(
            ((ng_hbm, ng), (sink_hbm, sink), (taps_hbm, taps), (cg_hbm, cg), (og_hbm, og))
        )
    ]
    loads[0].start()
    small[0].start()
    tloads[T - 1].start()
    for i in range(1, 6):
        loads[i].start()
    for q in range(T - 2, -1, -1):
        tloads[q].start()
    loads[6].start()
    for copy in small[1:]:
        copy.start()


    pl.semaphore_wait(bar, peers)

    other_x = s + 1 - 2 * x
    sib = y * 2 + 1 - c
    W0, W1, N = 0, 1, 2 + y
    M = [2 + lax.rem(y + k, Y) for k in range(1, Y)]
    groups = {}
    count = [0]
    conds = {}

    def cond_of(name, f):
        if name not in conds:
            conds[name] = f()
        return name

    def when(cond, f):
        if cond is None:
            f()
        else:
            pl.when(conds[cond])(f)

    front = z < Z // 2
    m = jnp.where(front, z, Z - 1 - z)

    def plane(r):
        spot = jnp.where(r <= 2 * m, m + (r // 2 if r % 2 == 0 else -(r + 1) // 2), r)
        return jnp.where(front, spot, Z - 1 - spot)

    def mine(r):
        return plane(r) * 2 + x

    def other(r):
        return plane(r) * 2 + 1 - x

    def onward(r):
        far = plane(r)
        return jnp.where(far < z, z + 1 < Z, z >= 1)

    def finishing(r):
        far = plane(r)
        up = (far == 0) & (z + 1 < Z) & (z + 1 >= Z // 2)
        down = (far == Z - 1) & (z >= 1) & (z - 1 < Z // 2)
        return up | down

    def unit(sh, u):
        rows = pl.ds(pl.multiple_of(sh * Kl, Kl), Kl)
        if isinstance(u, int) and u < 2:
            return wfull.at[rows, u * part : (u + 1) * part]
        return wfull.at[rows, pl.ds(pl.multiple_of(wide + (u - 2) * narrow, narrow), narrow)]

    def push(cond, src, dst, width, rsem, ds_, dt_):
        group = groups.setdefault(cond, [])
        if not group or group[-1][1] + width > half:
            group.append([count[0], 0])
            count[0] += 1
        group[-1][1] += width
        sem = wsend.at[group[-1][0]]

        def go():
            pltpu.make_async_remote_copy(
                src_ref=src, dst_ref=dst, send_sem=sem, recv_sem=rsem,
                device_id=(ds_, dt_), device_id_type=MESH,
            ).start()

        when(cond, go)

    def drain():
        for cond, group in groups.items():
            def wait(group=group):
                for i, width in group:
                    ref = wfull.at[0:Kl, 0:width]
                    pltpu.make_async_copy(ref, ref, wsend.at[i]).wait()

            when(cond, wait)

    def send(cond, sh, u, ds_, dt_):
        ref = unit(sh, u)
        width = part if isinstance(u, int) and u < 2 else narrow
        push(cond, ref, ref, width, wrecv.at[sh, u], ds_, dt_)

    def got(cond, sh, u):
        ref = unit(sh, u)
        when(cond, lambda: pltpu.make_async_copy(ref, ref, wrecv.at[sh, u]).wait())

    def to_x(cond, sh, u):
        send(cond, sh, u, other_x, t)

    def to_y(cond, sh):
        for k in range(1, Y):
            send(cond, sh, N, s, lax.rem(y + k, Y) * 2 + c)

    def z_out(sh, u):
        send(cond_of("up", lambda: z + 1 < Z), sh, u, s + 2, t)
        send(cond_of("down", lambda: z >= 1), sh, u, s - 2, t)

    def relay(r, u, oth=False):
        if not oth and not any(u is v for v in M):
            cond = cond_of(("onward", r), lambda: onward(r))
        else:
            cond = cond_of(("finishing", r), lambda: finishing(r))
        step = jnp.where(plane(r) < z, 2, -2)
        send(cond, other(r) if oth else mine(r), u, s + step, t)

    def plane_n(r, cond=None):
        got(cond, mine(r), N)
        if r < Z - 1:
            to_y(cond, mine(r))
            to_x(cond, mine(r), N)

    def plane_w(r, u, cond=None):
        got(cond, mine(r), u)
        to_x(cond, mine(r), u)

    def other_n(r, cond=None):
        got(cond, other(r), N)
        if r > 0:
            to_y(cond, other(r))

    def other_w(r, cond=None):
        got(cond, other(r), W0)
        got(cond, other(r), W1)

    def across(sh, cond=None):
        for u in M:
            got(cond, sh, u)

    def rest(r):
        other_w(r)
        if r != 1:
            across(mine(r))
        across(other(r))

    def inner():
        for r in range(3, last):
            for u in (N, W0, W1):
                (plane_n(r) if u is N else plane_w(r, u))
                relay(r, u)
            other_n(r)
            relay(r, N, True)
            across(mine(r))
            for u in M:
                relay(r, u)
            other_w(r)
            across(other(r))

    mid = cond_of("mid", lambda: (z > 0) & (z < Z - 1))
    end = cond_of("end", lambda: (z == 0) | (z == Z - 1))
    last = Z - 1

    loads[0].wait()
    for u in (N, W0):
        z_out(s, u)
        to_x(None, s, u)

    for i in range(1, 6):
        loads[i].wait()
    small[0].wait()
    wcat[:, HW : 2 * HW] = kvs[...].T

    def send_gated(q):
        rows = pl.ds(q * Q, HALO + Q)

        @pl.when(t != q)
        def _():
            pltpu.make_async_remote_copy(
                src_ref=g.at[rows], dst_ref=gr.at[t], send_sem=gsend.at[q], recv_sem=grecv.at[t],
                device_id=(s, q), device_id_type=MESH,
            ).start()

    def halo(ref, n, i):
        return pltpu.make_async_remote_copy(
            src_ref=ref.at[pl.ds(R, n)], dst_ref=ref.at[pl.ds(0, n)],
            send_sem=hsend.at[i], recv_sem=hrecv.at[i],
            device_id=(lax.rem(s + 1, S), t), device_id_type=MESH,
        )

    for q in range(T - 1, -1, -1):
        tloads[q].wait()
        xs = tok[q * Q : (q + 1) * Q, :].astype(F32)
        scale = lax.rsqrt(jnp.mean(xs * xs, axis=-1, keepdims=True) + EPS)
        normed = (xs * scale * ng[...]).astype(BF16)
        p = jnp.dot(normed, wcat[...], preferred_element_type=F32)
        qb[q * Q : (q + 1) * Q, :] = (p[:, :HW] * HEAD_DIM ** (-0.5)).astype(BF16)
        kvb[WINDOW + q * Q : WINDOW + (q + 1) * Q, :] = p[:, HW : 2 * HW].astype(BF16)
        g[HALO + q * Q : HALO + (q + 1) * Q, :] = (
            p[:, 2 * HW : 2 * HW + CC] * jax.nn.sigmoid(p[:, 2 * HW + CC :])
        ).astype(BF16)
        if q == T - 1:
            @pl.when(s + 1 < S)
            def _():
                halo(kvb, WINDOW, 0).start()
                halo(g, HALO, 1).start()
            z_out(s, W1)
            to_x(None, s, W1)
        else:
            send_gated(q + 1)
        if q == 1:
            plane_n(1)
            plane_n(2, mid)
            relay(2, N)

    small[1].wait()
    row = lax.broadcasted_iota(jnp.int32, (2 * WINDOW, 2 * WINDOW), 0)
    col = lax.broadcasted_iota(jnp.int32, (2 * WINDOW, 2 * WINDOW), 1)
    dist = WINDOW + lax.rem(row, WINDOW) - col
    inside = (dist >= 0) & (dist < WINDOW)
    head = lax.broadcasted_iota(jnp.int32, (2 * WINDOW, 1), 0) < WINDOW
    sinks = jnp.where(head, sink[0], sink[1])
    for copy in small[2:]:
        copy.wait()
    for i in range(T):
        if i < T - 2:
            q = 1 + lax.rem(t + i, T - 1)
        elif i == T - 2:
            q = (T - t) // T * (T - 1)
        else:
            q = t
        for b in range(Q // WINDOW):
            base = pl.multiple_of(q * Q + b * WINDOW, WINDOW)
            rows = qb[pl.ds(base, WINDOW), :]
            kv = kvb[pl.ds(base, 2 * WINDOW), :]
            q2 = jnp.concatenate([rows[:, :HEAD_DIM], rows[:, HEAD_DIM:]], axis=0)
            sc = lax.dot_general(
                q2, kv[:, :HEAD_DIM], (((1,), (1,)), ((), ())), preferred_element_type=F32
            )
            low = jnp.where((s == 0) & (base == 0), WINDOW, 0)
            sc = jnp.where(inside & (col >= low), sc, MASKED)
            top = jnp.maximum(jnp.max(sc, axis=-1, keepdims=True), sinks)
            e = jnp.exp(sc - top)
            den = jnp.sum(e, axis=-1, keepdims=True) + jnp.exp(sinks - top)
            w = (e * (1.0 / den)).astype(BF16)
            o = jnp.dot(w, kv[:, HEAD_DIM:], preferred_element_type=F32).astype(BF16)
            a[pl.ds(base, WINDOW), :] = jnp.concatenate([o[:WINDOW], o[WINDOW:]], axis=1)
        if i < T - 1:
            pltpu.make_async_remote_copy(
                src_ref=a.at[pl.ds(pl.multiple_of(q * Q, Q), Q)], dst_ref=ar.at[t],
                send_sem=asend.at[i], recv_sem=arecv.at[t],
                device_id=(s, q), device_id_type=MESH,
            ).start()
        if i == 0:
            @pl.when(s == 0)
            def _():
                kvb[0:WINDOW, :] = jnp.zeros((WINDOW, kvb.shape[1]), BF16)
                g[0:HALO, :] = jnp.zeros((HALO, CC), BF16)

            @pl.when(s > 0)
            def _():
                halo(kvb, WINDOW, 0).wait_recv()
                halo(g, HALO, 1).wait_recv()

            send_gated(0)
            for r, cond in ((1, None), (2, mid)):
                plane_w(r, W0, cond)
                relay(r, W0)
            relay(1, N)
        elif i == 1:
            for u in M:
                to_x(None, s, u)
        elif i == 2:
            for r, cond in ((1, None), (2, mid)):
                plane_w(r, W1, cond)
                relay(r, W1)
    own_rows = pl.multiple_of(t * Q, Q)
    ar[t] = a[pl.ds(own_rows, Q), :]
    gr[t] = g[pl.ds(own_rows, HALO + Q), :]
    other_n(1, mid)
    relay(1, N, True)
    across(mine(1))
    for u in M:
        relay(1, u)

    first = HALO - (CONV_WIDTH - 1)
    for j in range(T):
        k, b = j // 2, j % 2
        p = 2 * lax.rem(y + k, Y) + (c if b == 0 else 1 - c)
        if j > 0:
            pltpu.make_async_copy(gr.at[p], gr.at[p], grecv.at[p]).wait()
        cols = pl.ds(pl.multiple_of(p * CC, CC), CC)
        ext[j] = gr[p].astype(F32)
        total = jnp.zeros((Q, CC), F32)
        tp = taps[:, cols].astype(F32)
        for k in range(CONV_WIDTH):
            total = total + tp[k : k + 1] * ext[j, first + k : first + k + Q, :]
        conv[:, cols] = total.astype(BF16)
        if j == 1:
            plane_n(2, end)
            inner()
            plane_w(last, W0, mid)
            relay(last, W0)
            other_n(1, end)
            other_n(2, mid)
            plane_n(last, mid)
            relay(last, N)
        elif j == 2:
            plane_w(2, W0, end)
    plane_w(last, W1, mid)
    relay(last, W1)
    plane_w(2, W1, end)
    cv = conv[...].astype(F32)
    cen = cv - jnp.mean(cv, axis=-1, keepdims=True)
    norm = cen * lax.rsqrt(jnp.mean(cen * cen, axis=-1, keepdims=True) + EPS) * cg[...]
    act[...] = (norm * jax.nn.sigmoid(norm)).astype(BF16)
    loads[6].wait()
    pt = jnp.dot(act[...], pw[...], preferred_element_type=F32)
    AW = T * HW

    def swap(lo, hi, i):
        pltpu.make_async_remote_copy(
            src_ref=mg.at[0:Q, lo:hi], dst_ref=mg.at[Q : 2 * Q, lo:hi],
            send_sem=msend.at[i], recv_sem=mrecv.at[i],
            device_id=(s, sib), device_id_type=MESH,
        ).start()

    def swapped(lo, hi, i):
        ref = mg.at[Q : 2 * Q, lo:hi]
        pltpu.make_async_copy(ref, ref, mrecv.at[i]).wait()

    mg[0:Q, AW:] = (
        pt * lax.rsqrt(jnp.mean(pt * pt, axis=-1, keepdims=True) + EPS) * og[:, AW:]
    ).astype(BF16)
    swap(AW, mg.shape[1], 1)
    plane_w(last, W0, end)
    other_n(last, mid)
    relay(last, N, True)
    across(mine(last), mid)
    for u in M:
        relay(last, u)
    for d in range(1, T):
        p = lax.rem(t + d, T)
        pltpu.make_async_copy(ar.at[p], ar.at[p], arecv.at[p]).wait()
    heads = jnp.concatenate([ar[p] for p in range(T)], axis=1).astype(F32)
    mg[0:Q, :AW] = (
        heads * lax.rsqrt(jnp.mean(heads * heads, axis=-1, keepdims=True) + EPS) * og[:, :AW]
    ).astype(BF16)

    swap(0, AW, 0)

    nb = D // 8
    K2 = 2 * Kl
    tiled = K2 % 128 == 0
    upper, lower = slice(0, Q), slice(Q, 2 * Q)

    def term(r, rows, cols):
        ks = pl.ds(pl.multiple_of(plane(r) * K2, K2), K2)
        return jnp.dot(mg[rows, ks], wfull[ks, cols], preferred_element_type=F32)

    def blocks():
        return [slice(n * nb, (n + 1) * nb) for n in range(half // nb)]

    other_n(2, end)
    plane_n(last, end)
    other_n(0)
    other_w(0)
    across(other(0))
    rest(1)
    plane_w(last, W1, end)
    swapped(AW, mg.shape[1], 1)
    swapped(0, AW, 0)
    if tiled:
        for cols in blocks():
            acc[:, cols] = term(0, slice(None), cols) + term(1, slice(None), cols)
    other_n(last, end)
    rest(2)
    if tiled:
        for r in range(2, Z - 1):
            for cols in blocks():
                acc[:, cols] += term(r, slice(None), cols)
    def total(rows, cols):
        if tiled:
            return (acc[rows, cols] + term(Z - 1, rows, cols)).astype(BF16)
        return jnp.dot(mg[rows, :], wfull[:, cols], preferred_element_type=F32).astype(BF16)

    def landing(cc, cols):
        start = pl.multiple_of(cc * half + cols.start, nb)
        return out.at[:, pl.ds(start, cols.stop - cols.start)]

    outs = []

    def finish(cols):
        i = len(outs)
        both = total(slice(None), cols)
        theirs[:, cols] = both[lower]
        landing(c, cols)[...] = both[upper]
        copy = pltpu.make_async_remote_copy(
            src_ref=theirs.at[:, cols], dst_ref=landing(c, cols),
            send_sem=osend.at[i], recv_sem=orecv.at[i],
            device_id=(s, sib), device_id_type=MESH,
        )
        copy.start()
        outs.append((copy, cols))

    across(mine(last), end)
    across(other(last))
    if not tiled:
        other_w(Z - 1)
    finish(slice(wide, half))
    for u in (W0, W1):
        if tiled:
            got(None, other(Z - 1), u)
        finish(slice(u * part, (u + 1) * part))
    drain()

    @pl.when(s + 1 < S)
    def _():
        halo(kvb, WINDOW, 0).wait_send()
        halo(g, HALO, 1).wait_send()

    for q in range(T):
        @pl.when(t != q)
        def _():
            pltpu.make_async_copy(gr.at[0], gr.at[0], gsend.at[q]).wait()
    for i in range(T - 1):
        pltpu.make_async_copy(ar.at[0], ar.at[0], asend.at[i]).wait()
    for i, (lo, hi) in enumerate(((0, AW), (AW, mg.shape[1]))):
        ref = mg.at[0:Q, lo:hi]
        pltpu.make_async_copy(ref, ref, msend.at[i]).wait()
    for i, (copy, cols) in enumerate(outs):
        copy.wait_send()
        ref = landing(1 - c, cols)
        pltpu.make_async_copy(ref, ref, orecv.at[i]).wait()


def solution(mesh):
    S, T = mesh.shape["sp"], mesh.shape["tp"]

    def step(
        tokens, norm_gain, query_weight, key_weight, value_weight, sink_logits, conv_in_weight,
        conv_gate_weight, conv_taps, conv_gain, point_weight, output_gain, output_weight,
    ):
        R, D = tokens.shape
        Q = R // T
        HW, KW, CC = query_weight.shape[1], key_weight.shape[1], conv_in_weight.shape[1]
        C = point_weight.shape[0]
        MIX = output_gain.shape[0]
        Y, Z = T // 2, S // 2
        hbm = pl.BlockSpec(memory_space=pl.ANY)
        vmem = pl.BlockSpec(memory_space=pltpu.VMEM)
        dma = pltpu.SemaphoreType.DMA
        return pl.pallas_call(
            functools.partial(kernel, S, T),
            out_shape=pltpu.VMEM((Q, D), BF16),
            in_specs=[hbm] * 13,
            out_specs=vmem,
            scratch_shapes=[
                pltpu.VMEM((R, D), BF16),
                pltpu.VMEM((D, HW + 2 * KW + 2 * CC), BF16),
                pltpu.VMEM((2 * KW, D), BF16),
                pltpu.VMEM((C, C), BF16),
                pltpu.VMEM((MIX, D // 2), BF16),
                pltpu.VMEM((R, HW), BF16),
                pltpu.VMEM((R + WINDOW, 2 * KW), BF16),
                pltpu.VMEM((R + HALO, CC), BF16),
                pltpu.VMEM((R, HW), BF16),
                pltpu.VMEM((T, Q, HW), BF16),
                pltpu.VMEM((T, Q + HALO, CC), BF16),
                pltpu.VMEM((T, Q + HALO, CC), F32),
                pltpu.VMEM((Q, C), BF16),
                pltpu.VMEM((Q, C), BF16),
                pltpu.VMEM((2 * Q, MIX), BF16),
                pltpu.VMEM((2 * Q, D // 2), F32),
                pltpu.VMEM((Q, D // 2), BF16),
                pltpu.VMEM((1, D), F32),
                pltpu.SMEM(sink_logits.shape, F32),
                pltpu.VMEM(conv_taps.shape, BF16),
                pltpu.VMEM((1, C), F32),
                pltpu.VMEM((1, MIX), F32),
                dma((12 + T,)),
                dma((8 * Z + 16,)),
                dma((S, Y + 2)),
                dma((2,)),
                dma((2,)),
                dma((T,)),
                dma((T,)),
                dma((T,)),
                dma((T,)),
                dma((2,)),
                dma((2,)),
                dma((4,)),
                dma((4,)),
            ],
            compiler_params=pltpu.CompilerParams(
                collective_id=0, has_side_effects=True, vmem_limit_bytes=56 * 1024 * 1024
            ),
        )(
            tokens, norm_gain[None], query_weight, key_weight.T, value_weight.T, sink_logits,
            conv_in_weight, conv_gate_weight, conv_taps, conv_gain[None], point_weight,
            output_gain[None], output_weight,
        )

    in_specs = (
        P("sp", None), P(), P(None, "tp"), P(None, "tp"), P(None, "tp"), P("tp"), P(None, "tp"),
        P(None, "tp"), P(), P(), P(), P(), P("sp", None),
    )
    return jax.shard_map(
        step, mesh=mesh, in_specs=in_specs, out_specs=P(("sp", "tp"), None), check_vma=False
    )
```

time: 33.7 us -> 29.3 us (0.87)
  the two profiles are of different devices: /device:TPU:1 before, /device:TPU:0 now
where the time goes in v1:
time: 29.3 us; the launch traced here: 29.2 us
  Pallas kernels  28.2 us (96%)
  local copies, waits for them, and re-layouts  0.97 us (3%)
    pallas_call x1, Pallas kernels, step(): pl.pallas_call(functools.partial(kernel, S, T), out_shape=pltpu.VMEM((Q,...  28.2 us
    unnamed x1, local copies, waits for them, and re-layouts  0.97 us

profile of v1, /device:TPU:0, one launch (start us, length us, event | category | flops | bytes accessed | tf_op | source)
XLA Modules:
  0.0 29.2 jit_solution(14830815713039854328)
XLA Ops:
  0.0 28.2 %shard_map.127 = bf16[256,2048]{1,0:T(8,128)(2,1)S(1)} custom-call(bf16[1024,2048]{1,0:T(8,128)(2,1)} %tok_hbm.1, f32[1,2048]{1,0:T(1,128)} %bitcast.7, bf16[2048,128]{1,0:T(8,128)(2,1)} %qw.1, bf16[64,2048]{1,0:T(8,128)(2,1)} %bitcast.5, bf16[64,2048]{1,0:T(8,128)(2,1)} %bitcast.6, f32[2]{0:T(128)} %sink_hbm.1, bf16[2048,128]{1,0:T(8,128)(2,1)} %iw.1, ...), custom_call_target="tpu_custom_call" | custom-call | tf_op jit(solution)/shard_map/pallas_call | solution.py:530
  28.2 1.0 %copy.15 = bf16[256,2048]{1,0:T(8,128)(2,1)} copy(bf16[256,2048]{1,0:T(8,128)(2,1)S(1)} %shard_map.127) | data formatting | bytes 2097152
